TPU v7x, 512 devices: a whole 4x4x16 slice. The times are simulated.
512 devices in a mesh: ep: 128 (over z, x, core), tp: 4 (over y).
Axes of the slice: x: 4, y: 4, z: 16, core: 2. Of those that a mesh axis runs over, the one named last changes fastest.
Arguments:
- tokens: bfloat16 [2048, 1024], P('ep'), may hold values from -6 to 6
- memory: float32 [2048, 4, 128, 256], P('ep', 'tp'), may hold values from -6 to 6
- log_scale: float32 [2048, 4], P('ep', 'tp'), may hold values from -1 to 130
- mix_gain_in: float32 [1024], replicated, may hold values from 0.1 to 1.9
- w_query: bfloat16 [1024, 512], P(None, 'tp'), may hold values from -0.1875 to 0.1875
- w_key: bfloat16 [1024, 512], P(None, 'tp'), may hold values from -0.1875 to 0.1875
- w_value: bfloat16 [1024, 1024], P(None, 'tp'), may hold values from -0.1875 to 0.1875
- w_igate: bfloat16 [1024, 4], P(None, 'tp'), may hold values from -0.1875 to 0.1875
- w_fgate: bfloat16 [1024, 4], P(None, 'tp'), may hold values from -0.1875 to 0.1875
- igate_bias: float32 [4], P('tp'), may hold values from -1 to 1
- fgate_bias: float32 [4], P('tp'), may hold values from 0 to 4
- head_gain: float32 [1024], P('tp'), may hold values from 0.1 to 1.9
- w_output: bfloat16 [1024, 1024], P('tp'), may hold values from -0.1875 to 0.1875
- mix_gain_out: float32 [1024], replicated, may hold values from 0.1 to 1.9
- ffn_gain_in: float32 [1024], replicated, may hold values from 0.1 to 1.9
- routes: int32 [2048, 6], P('ep'), may hold values from 0 to 127, all different within a row; in each aligned block of 16 rows (0 to 15, 16 to 31, ...) at most 2 rows name the same one
- route_weights: float32 [2048, 6], P('ep'), may hold values from 0.1 to 1
- expert_gate: bfloat16 [128, 1024, 1024], P('ep', None, 'tp'), may hold values from -0.1875 to 0.1875
- expert_up: bfloat16 [128, 1024, 1024], P('ep', None, 'tp'), may hold values from -0.1875 to 0.1875
- expert_down: bfloat16 [128, 1024, 1024], P('ep', 'tp'), may hold values from -0.9375 to 0.9375
- ffn_gain_out: float32 [1024], P('tp'), may hold values from 0.1 to 1.9
Outputs:
- output: bfloat16 [2048, 1024], P('ep', 'tp')
Inputs may be any that keep to these rules, and one draw needn't show every extreme that they name: `routes`: among the 16 tokens of one index of ep no expert is named by more than 2 tokens, and in every draw some expert is named by exactly 2 of them.
All inputs are finite; a program needn't handle non-finite values.
Results may differ from a plain program's by a relative error of at most 0.02.
Values may be sent and summed in bfloat16 or wider, within the bound.
A program may use at most 64 MiB of HBM per device.

v0:
```python
import jax
import jax.numpy as jnp
from jax import lax
from jax.sharding import PartitionSpec as P

EPS = 1e-06


def from_everyone(array, axis):
    size = lax.axis_size(axis)
    return lax.all_to_all(
        jnp.broadcast_to(array[None], (size, *array.shape)), axis, 0, 0, tiled=True
    )


def over_copies(array, axis):
    return from_everyone(array, axis).astype(jnp.float32).sum(axis=0)


def in_blocks(array, dim, size):
    dims = array.shape
    blocks = array.reshape(*dims[:dim], size, dims[dim] // size, *dims[dim + 1 :])
    return jnp.moveaxis(blocks, dim, 0)


def summed_on_arrival(array, axis, dim):
    blocks = in_blocks(array, dim, lax.axis_size(axis))
    arrived = lax.all_to_all(blocks, axis, split_axis=0, concat_axis=0, tiled=True)
    return arrived.astype(jnp.float32).sum(axis=0)


def laid_out(blocks, dim):
    dims = list(blocks.shape[1:])
    dims[dim] *= blocks.shape[0]
    return jnp.moveaxis(blocks, 0, dim).reshape(dims)


def gathered_copies(array, axis, dim):
    blocks = from_everyone(array, axis)
    return laid_out(blocks, dim)


def of_everyone(array, axis):
    everything = from_everyone(array, axis)
    return jnp.sum(everything, axis=0)


def rms_scale(values):
    return lax.rsqrt(jnp.mean(values * values, axis=-1, keepdims=True) + EPS)


def per_device(
    tokens,
    memory,
    log_scale,
    mix_gain_in,
    w_query,
    w_key,
    w_value,
    w_igate,
    w_fgate,
    igate_bias,
    fgate_bias,
    head_gain,
    w_output,
    mix_gain_out,
    ffn_gain_in,
    routes,
    route_weights,
    expert_gate,
    expert_up,
    expert_down,
    ffn_gain_out,
):
    f32 = jnp.float32
    bf16 = jnp.bfloat16
    seqs, width = tokens.shape
    heads = log_scale.shape[1]
    key_dim = memory.shape[2]
    value_dim = memory.shape[3]
    xf = tokens.astype(f32)
    normed = (xf * rms_scale(xf) * mix_gain_in).astype(bf16)
    query = jnp.dot(normed, w_query, preferred_element_type=f32).reshape(
        seqs, heads, key_dim
    ) * key_dim ** (-0.5)
    keys = jnp.dot(normed, w_key, preferred_element_type=f32).reshape(seqs, heads, key_dim)
    values = jnp.dot(normed, w_value, preferred_element_type=f32).reshape(seqs, heads, value_dim)
    in_pre = jnp.dot(normed, w_igate, preferred_element_type=f32) + igate_bias
    forget_log = jax.nn.log_sigmoid(
        jnp.dot(normed, w_fgate, preferred_element_type=f32) + fgate_bias
    )
    carried = forget_log + log_scale
    new_max = jnp.maximum(carried, in_pre)
    carry_weight = jnp.exp(carried - new_max)
    fresh_weight = jnp.exp(in_pre - new_max)
    recall = jnp.einsum("shk,shkv->shv", query, memory)
    match = jnp.sum(query * keys, axis=-1)
    read = carry_weight[..., None] * recall + (fresh_weight * match)[..., None] * values
    headout = (
        (read * rms_scale(read) * head_gain.reshape(heads, value_dim))
        .astype(bf16)
        .reshape(seqs, heads * value_dim)
    )
    partial_value = jnp.dot(headout, w_output, preferred_element_type=f32)
    mixed = over_copies(partial_value.astype(jnp.bfloat16), "tp").astype(jnp.float32)
    resid = (xf + mixed * rms_scale(mixed) * mix_gain_out).astype(bf16)
    rf = resid.astype(f32)
    ffn_in = (rf * rms_scale(rf) * ffn_gain_in).astype(bf16)
    lanes = lax.axis_size("tp")
    quarter = width // lanes
    own = lax.axis_index("tp") * quarter
    local_experts = expert_gate.shape[0]
    experts_all = local_experts * lax.axis_size("ep")
    top = routes.shape[1]
    cap = min(seqs, max(2, 3 * seqs * top // (2 * experts_all)))
    flat = routes.reshape(-1)
    hits = (flat[:, None] == jnp.arange(experts_all, dtype=jnp.int32)[None, :]).astype(jnp.int32)
    earlier = jnp.cumsum(hits, axis=0) - hits
    slot = jnp.sum(earlier * hits, axis=1)
    place = (flat * cap + slot).reshape(seqs, top)
    picker = jnp.any(
        jnp.arange(experts_all * cap, dtype=jnp.int32)[:, None, None] == place[None, :, :], axis=2
    ).astype(bf16)
    piece = lax.dynamic_slice_in_dim(ffn_in, own, quarter, 1)
    outbound = (
        jnp.dot(picker, piece, preferred_element_type=f32)
        .astype(bf16)
        .reshape(experts_all, cap, quarter)
    )
    arrived = gathered_copies(
        lax.all_to_all(outbound, "ep", split_axis=0, concat_axis=0, tiled=True), "tp", 2
    )
    items = arrived.shape[1]
    rows = arrived.reshape(-1, local_experts, items, width)
    gate = jnp.einsum("secd,edf->secf", rows, expert_gate, preferred_element_type=f32)
    up = jnp.einsum("secd,edf->secf", rows, expert_up, preferred_element_type=f32)
    act = (jax.nn.silu(gate) * up).astype(bf16)
    part = jnp.einsum("secf,efd->secd", act, expert_down, preferred_element_type=f32).reshape(
        -1, items, width
    )
    summed = summed_on_arrival(part.astype(jnp.bfloat16), "tp", 2)
    done = summed.astype(bf16)
    returned = lax.all_to_all(done, "ep", split_axis=0, concat_axis=0, tiled=True)
    columns = returned.shape[2]
    chosen = jnp.take(returned.reshape(-1, columns), place.reshape(-1), axis=0).reshape(
        seqs, top, columns
    )
    routed = jnp.sum(route_weights[:, :, None] * chosen.astype(f32), axis=1)
    resid_part = lax.dynamic_slice_in_dim(rf, own, quarter, 1)
    total = of_everyone(jnp.sum(routed * routed, axis=1), "tp")
    scaled = routed * lax.rsqrt(total / width + EPS)[:, None]
    return (resid_part + scaled * ffn_gain_out).astype(bf16)


def solution(mesh):
    return jax.shard_map(
        per_device,
        mesh=mesh,
        in_specs=(
            P("ep", None),
            P("ep", "tp", None, None),
            P("ep", "tp"),
            P(),
            P(None, "tp"),
            P(None, "tp"),
            P(None, "tp"),
            P(None, "tp"),
            P(None, "tp"),
            P("tp"),
            P("tp"),
            P("tp"),
            P("tp", None),
            P(),
            P(),
            P("ep", None),
            P("ep", None),
            P("ep", None, "tp"),
            P("ep", None, "tp"),
            P("ep", "tp", None),
            P("tp"),
        ),
        out_specs=P("ep", "tp"),
        check_vma=False,
    )
```

profile of v0, /device:TPU:1, one launch (start us, length us, event | category | flops | bytes accessed | tf_op | source)
XLA Modules:
  0.0 114.2 jit_solution(6009987493279582933)
XLA Ops:
  0.1 1.0 fusion.23
  2.4 1.2 %convolution_multiply_fusion.2 = f32[16,128]{1,0:T(8,128)S(1)} fusion(bf16[1024,128]{1,0:T(8,128)(2,1)} %param.25, bf16[16,1024]{1,0:T(8,128)(2,1)} %param.21, f32[1024]{0:T(1024)} %param.24, f32[16]{0:T(128)S(1)} %add_rsqrt_fusion.4), kind=kOutput, calls=%fused_computation.15 | convolution fusion | flops 4261888 | bytes 307264 | tf_op jit(solution)/shard_map/dot_general | solution.py:83
  3.6 1.3 %fusion.7 = f32[16]{0:T(128)S(1)} fusion(f32[16,128]{1,0:T(8,128)S(1)} %convolution_multiply_fusion.2, bf16[1024,128]{1,0:T(8,128)(2,1)} %param.26, bf16[16,1024]{1,0:T(8,128)(2,1)} %param.21, f32[1024]{0:T(1024)} %param.24, f32[16]{0:T(128)S(1)} %add_rsqrt_fusion.4), kind=kOutput, calls=%fused_computation.16 | convolution fusion | flops 4263920 | bytes 307328 | tf_op jit(solution)/shard_map/dot_general | solution.py:86
  4.9 1.0 fusion.9
  5.9 0.3 fusion.51
  6.2 0.0 copy-done.12
  6.2 0.2 fusion.38
  6.4 0.3 multiply_reduce_fusion.4
  6.8 0.2 convolution_convert_fusion.2
  7.0 0.7 broadcast_in_dim.13
  7.7 5.0 %all-to-all-start = ((bf16[4,16,1024]{2,1,0:T(8,128)(2,1)}), bf16[4,16,1024]{2,1,0:T(8,128)(2,1)S(1)}, u32[]{:S(2)}, u32[]{:S(2)}) async-start(bf16[4,16,1024]{2,1,0:T(8,128)(2,1)} %broadcast_in_dim.13), calls=%async_computation | async-start | bytes 262144 | tf_op jit(solution)/shard_map/all_to_all | solution.py:11
  12.7 0.1 copy.56
  12.7 0.1 reshape.198
  12.8 0.1 fusion.27
  12.9 0.1 reduce_window_sum.11
  13.1 0.2 select_reduce_fusion
  13.2 0.1 reduce_sum.115
  13.3 0.0 copy-start.2
  13.4 0.1 copy.58
  13.4 0.8 dynamic-slice
  14.2 0.1 fusion.22
  14.3 3.2 %all-to-all-done = bf16[4,16,1024]{2,1,0:T(8,128)(2,1)S(1)} async-done(((bf16[4,16,1024]{2,1,0:T(8,128)(2,1)}), bf16[4,16,1024]{2,1,0:T(8,128)(2,1)S(1)}, u32[]{:S(2)}, u32[]{:S(2)}) %all-to-all-start) | async-done | bytes 131104 | tf_op jit(solution)/shard_map/all_to_all | solution.py:11
  17.5 0.1 multiply_reduce_fusion.2
  17.6 0.2 multiply_reduce_fusion.1
  17.9 0.3 convolution_convert_fusion.1
  18.1 0.1 reshape.199
  18.2 37.1 %all_to_all.31 = bf16[128,2,256]{2,1,0:T(2,128)(2,1)S(1)} all-to-all(bf16[128,2,256]{2,1,0:T(2,128)(2,1)S(1)} %reshape.199), channel_id=1, replica_groups=mesh['ep'=128,'tp'=4] {'ep'}, dimensions={0} | all-to-all | bytes 262144 | tf_op jit(solution)/shard_map/all_to_all | solution.py:131
  55.4 11.6 %all_to_all.32 = bf16[4,128,2,256]{3,1,2,0:T(8,128)(2,1)S(1)} all-to-all(bf16[4,128,2,256]{3,1,2,0:T(8,128)(2,1)S(1)} %broadcast_in_dim.15), channel_id=1, replica_groups=mesh['ep'=128,'tp'=4] {'tp'}, dimensions={0} | all-to-all | bytes 1048576 | tf_op jit(solution)/shard_map/all_to_all | solution.py:11
  66.9 0.1 copy.68
  67.0 0.3 convolution_bitcast_fusion.1
  67.3 1.9 %fusion.2 = bf16[128,1,2,1024]{3,0,2,1:T(8,128)(2,1)S(1)} fusion(bf16[128,2,1024]{2,0,1:T(8,128)(2,1)S(1)} %bitcast.124, bf16[1,256,1024]{2,1,0:T(8,128)(2,1)} %param.40, bf16[1,1024,256]{2,1,0:T(8,128)(2,1)} %param.39, f32[128,1,2,256]{3,0,2,1:T(8,128)S(1)} %convolution_bitcast_fusion.1), kind=kOutput, calls=%fused_computation.4 | convolution fusion | flops 269090816 | bytes 2359296 | tf_op jit(solution)/shard_map/secf,efd->secd/dot_general | solution.py:138
  69.3 0.0 copy-start.5
  69.3 0.4 convert_element_type.74
  69.7 0.0 copy-start.8
  69.7 0.1 copy.71
  69.8 10.7 %all_to_all.33 = bf16[4,128,2,256]{3,1,2,0:T(8,128)(2,1)S(1)} all-to-all(bf16[4,128,2,256]{3,1,2,0:T(8,128)(2,1)S(1)} %bitcast.126), channel_id=1, replica_groups=mesh['ep'=128,'tp'=4] {'tp'}, dimensions={0} | all-to-all | bytes 1048576 | tf_op jit(solution)/shard_map/all_to_all | solution.py:28
  80.5 0.1 reduce_sum.117
  80.6 0.8 copy.63
  81.3 8.5 %all-to-all-start.4 = ((bf16[128,2,256]{2,1,0:T(2,128)(2,1)}), bf16[128,2,256]{2,1,0:T(2,128)(2,1)S(1)}, u32[]{:S(2)}, u32[]{:S(2)}) async-start(bf16[128,2,256]{2,1,0:T(2,128)(2,1)} %copy.63), calls=%async_computation.4 | async-start | bytes 262144 | tf_op jit(solution)/shard_map/all_to_all | solution.py:143
  89.9 0.1 mul.213
  90.0 0.1 copy.55
  90.1 15.8 %all-to-all-done.4 = bf16[128,2,256]{2,1,0:T(2,128)(2,1)S(1)} async-done(((bf16[128,2,256]{2,1,0:T(2,128)(2,1)}), bf16[128,2,256]{2,1,0:T(2,128)(2,1)S(1)}, u32[]{:S(2)}, u32[]{:S(2)}) %all-to-all-start.4) | async-done | bytes 131104 | tf_op jit(solution)/shard_map/all_to_all | solution.py:143
  105.9 0.1 reshape.205
  105.9 0.8 gather_fusion
  106.7 0.1 multiply_reduce_fusion
  106.9 0.1 multiply_reduce_fusion.3
  107.0 6.5 %all_to_all.34 = f32[4,1,16]{2,1,0:T(1,128)S(1)} all-to-all(f32[4,1,16]{2,1,0:T(1,128)S(1)} %broadcast_in_dim.17), channel_id=1, replica_groups=mesh['ep'=128,'tp'=4] {'tp'}, dimensions={0} | all-to-all | bytes 512 | tf_op jit(solution)/shard_map/all_to_all | solution.py:11
  113.5 0.7 add_convert_fusion
  (37 shorter events, 0.2 us)
Async XLA Ops:
  0.0 5.9 %copy-start = (f32[16,1,128,256]{3,2,1,0:T(8,128)S(1)}, f32[16,1,128,256]{3,2,1,0:T(8,128)}, u32[]{:S(2)}) copy-start(f32[16,1,128,256]{3,2,1,0:T(8,128)} %param.22) | copy-start | bytes 6291460
  0.0 6.2 %copy-start.3 = (bf16[16,1024]{1,0:T(8,128)(2,1)S(1)}, bf16[16,1024]{1,0:T(8,128)(2,1)}, u32[]{:S(2)}) copy-start(bf16[16,1024]{1,0:T(8,128)(2,1)} %param.21) | copy-start | bytes 98308
  0.0 6.2 %copy-start.11 = (f32[1024]{0:T(1024)S(1)}, f32[1024]{0:T(1024)}, u32[]{:S(2)}) copy-start(f32[1024]{0:T(1024)} %param.24) | copy-start | bytes 12292
  0.0 6.2 %copy-start.12 = (f32[16,1]{0,1:T(1,128)S(1)}, f32[16,1]{0,1:T(1,128)}, u32[]{:S(2)}) copy-start(f32[16,1]{0,1:T(1,128)} %param.23) | copy-start | bytes 196
  0.0 6.2 %copy-start.10 = (bf16[1024,1]{0,1:T(2,128)(2,1)S(1)}, bf16[1024,1]{0,1:T(2,128)(2,1)}, u32[]{:S(2)}) copy-start(bf16[1024,1]{0,1:T(2,128)(2,1)} %param.29) | copy-start | bytes 6148
  0.0 6.4 %copy-start.9 = (bf16[1024,256]{1,0:T(8,128)(2,1)S(1)}, bf16[1024,256]{1,0:T(8,128)(2,1)}, u32[]{:S(2)}) copy-start(bf16[1024,256]{1,0:T(8,128)(2,1)} %param.27) | copy-start | bytes 1572868
  0.0 6.7 %copy-start.7 = (f32[256]{0:T(256)S(1)}, f32[256]{0:T(256)}, u32[]{:S(2)}) copy-start(f32[256]{0:T(256)} %param.32) | copy-start | bytes 3076
  0.1 6.7 %copy-start.1 = (bf16[256,1024]{1,0:T(8,128)(2,1)S(1)}, bf16[256,1024]{1,0:T(8,128)(2,1)}, u32[]{:S(2)}) copy-start(bf16[256,1024]{1,0:T(8,128)(2,1)} %param.33) | copy-start | bytes 1572868
  3.6 9.1 %copy-start.4 = (s32[16,6]{0,1:T(8,128)S(1)}, s32[16,6]{0,1:T(8,128)}, u32[]{:S(2)}) copy-start(s32[16,6]{0,1:T(8,128)} %param.36) | copy-start | bytes 1156
  5.9 11.7 %copy-start.6 = (f32[1024]{0:T(1024)S(1)}, f32[1024]{0:T(1024)}, u32[]{:S(2)}) copy-start(f32[1024]{0:T(1024)} %param.34) | copy-start | bytes 12292
  7.7 9.8 %all-to-all-start = ((bf16[4,16,1024]{2,1,0:T(8,128)(2,1)}), bf16[4,16,1024]{2,1,0:T(8,128)(2,1)S(1)}, u32[]{:S(2)}, u32[]{:S(2)}) async-start(bf16[4,16,1024]{2,1,0:T(8,128)(2,1)} %broadcast_in_dim.13), calls=%async_computation | async-start | bytes 262144 | tf_op jit(solution)/shard_map/all_to_all | solution.py:11
  13.3 53.7 %copy-start.2 = (bf16[1,1024,256]{2,1,0:T(8,128)(2,1)S(1)}, bf16[1,1024,256]{2,1,0:T(8,128)(2,1)}, u32[]{:S(2)}) copy-start(bf16[1,1024,256]{2,1,0:T(8,128)(2,1)} %param.38) | copy-start | bytes 1572868
  69.3 20.7 %copy-start.5 = (f32[16,6]{0,1:T(8,128)S(1)}, f32[16,6]{0,1:T(8,128)}, u32[]{:S(2)}) copy-start(f32[16,6]{0,1:T(8,128)} %param.37) | copy-start | bytes 1156
  69.7 43.8 %copy-start.8 = (f32[256]{0:T(256)S(1)}, f32[256]{0:T(256)}, u32[]{:S(2)}) copy-start(f32[256]{0:T(256)} %param.41) | copy-start | bytes 3076
  81.3 24.5 %all-to-all-start.4 = ((bf16[128,2,256]{2,1,0:T(2,128)(2,1)}), bf16[128,2,256]{2,1,0:T(2,128)(2,1)S(1)}, u32[]{:S(2)}, u32[]{:S(2)}) async-start(bf16[128,2,256]{2,1,0:T(2,128)(2,1)} %copy.63), calls=%async_computation.4 | async-start | bytes 262144 | tf_op jit(solution)/shard_map/all_to_all | solution.py:143
where the time goes:
time: 116 us; the launch traced here: 114 us
  blocking collectives  65.9 us (57%)
  waiting for transfers between devices  18.9 us (16%)
  starting transfers between devices  13.5 us (12%)
  matrix products  6.99 us (6%)
  local copies, waits for them, and re-layouts  4.28 us (4%)
  other arithmetic  2.92 us (3%)
  between operations  1.61 us (1%)
    all_to_all x1, blocking collectives, per_device(): lax.all_to_all(outbound, 'ep', split_axis=0, concat_axis=0, tiled=True)  37.1 us
    all_to_all x2, blocking collectives, from_everyone(): lax.all_to_all(jnp.broadcast_to(array[None], (size, *array.shape)), axis,...  18.1 us
    all_to_all x1, waiting for transfers between devices, per_device(): lax.all_to_all(done, 'ep', split_axis=0, concat_axis=0, tiled=True)  15.8 us
    all_to_all x1, blocking collectives, summed_on_arrival(): lax.all_to_all(blocks, axis, split_axis=0, concat_axis=0, tiled=True)  10.7 us
    all_to_all x1, starting transfers between devices, per_device(): lax.all_to_all(done, 'ep', split_axis=0, concat_axis=0, tiled=True)  8.52 us
    all_to_all x1, starting transfers between devices, from_everyone(): lax.all_to_all(jnp.broadcast_to(array[None], (size, *array.shape)), axis,...  5 us
    all_to_all x1, waiting for transfers between devices, from_everyone(): lax.all_to_all(jnp.broadcast_to(array[None], (size, *array.shape)), axis,...  3.15 us
  transfers between devices with their start and end apart: 2, of which 2 were waited for; matrix products, arithmetic and copies ran while one was open for 2% of the time, Pallas kernels for 0%

commit v1 on v0

v1 whole, which is shorter than its diff:
```python
import functools

import jax
import jax.numpy as jnp
from jax import lax
from jax.experimental import pallas as pl
from jax.experimental.pallas import tpu as pltpu
from jax.sharding import PartitionSpec as P

EPS = 1e-06
MESH = pl.DeviceIdType.MESH
LANES = 128
NX = 4
NY = 4
CHUNKS = 4


def offset_of(rank):
    return (rank + 1) // 2 if rank % 2 else -(rank // 2)


def rms(values):
    return lax.rsqrt(jnp.mean(values * values, axis=-1, keepdims=True) + EPS)


def kernel(
    nz,
    tokens_h, memory_h, scale_h, gain_in_h, wq_h, wk_h, wv_h, wi_h, wf_h, bi_h, bf_h,
    head_gain_h, wo_h, gain_out_h, gain_ffn_h, routes_h, weights_h, eg_h, eu_h, ed_h, gain_last_h,
    out_ref,
    tokens_v, memory_v, scale_v, gain_in_v, wq_v, wk_v, wv_v, wi_v, wf_v, bi_v, bf_v,
    head_gain_v, wo_v, gain_out_v, gain_ffn_v, routes_v, weights_v, eg_v, eu_v, ed_v, gain_last_v,
    recall_v, mix_v, pick_v, pull_hi_v, pull_lo_v, msg_v, rows_v, part_v, red_v, back_v, home_v, last_v, resid_v, total_v,
    load_sem, mix_send, mix_recv, out_send, self_send, in_recv, self_recv, gat_send, gat_recv,
    red_send, red_recv, ret_send, ret_self_send, ret_recv, ret_self_recv, last_send, last_recv,
):
    f32, bf16 = jnp.float32, jnp.bfloat16
    seqs, width = tokens_v.shape
    pieces = width // LANES
    slots = 2 * nz
    per = slots // CHUNKS
    experts = nz * NX * 2

    me = lax.axis_index("ep")
    y = lax.axis_index("tp")
    c = me % 2
    x = (me // 2) % NX
    z = me // (2 * NX)
    px = (y + NX - x) % NX
    mine = px == x

    def target(slot, sign):
        zz = (z + nz + sign * offset_of(slot // 2)) % nz
        cc = c if slot % 2 == 0 else 1 - c
        return (zz * NX + px) * 2 + cc

    def peer(step):
        return (y + step) % NY

    pairs = [
        (routes_h, routes_v), (weights_h, weights_v), (tokens_h, tokens_v), (gain_in_h, gain_in_v),
        (wq_h, wq_v), (wk_h, wk_v), (wv_h, wv_v), (wi_h, wi_v), (wf_h, wf_v), (bi_h, bi_v), (bf_h, bf_v),
        (scale_h, scale_v), (memory_h, memory_v), (head_gain_h, head_gain_v), (wo_h, wo_v),
        (gain_out_h, gain_out_v), (gain_ffn_h, gain_ffn_v), (eg_h, eg_v), (eu_h, eu_v), (ed_h, ed_v),
        (gain_last_h, gain_last_v),
    ]
    loads = {}
    for i, (src, dst) in enumerate(pairs):
        loads[id(dst)] = pltpu.make_async_copy(src, dst, load_sem.at[i])
        loads[id(dst)].start()

    def ready(*refs):
        for ref in refs:
            loads[id(ref)].wait()

    barrier = pltpu.get_barrier_semaphore()
    for step in range(1, NY):
        pl.semaphore_signal(barrier, inc=1, device_id=(me, peer(step)), device_id_type=MESH)
    for slot in range(1, slots):
        pl.semaphore_signal(barrier, inc=1, device_id=(target(slot, 1), y), device_id_type=MESH)

    @pl.when(jnp.logical_not(mine))
    def _():
        pl.semaphore_signal(barrier, inc=1, device_id=(target(0, 1), y), device_id_type=MESH)

    ready(routes_v, weights_v)
    expert_row = lax.broadcasted_iota(jnp.int32, (experts, LANES), 0)
    named = jnp.zeros((experts, LANES), f32)
    weight = jnp.zeros((experts, LANES), f32)
    for j in range(routes_v.shape[0]):
        hit = expert_row == routes_v[j : j + 1, :]
        named = jnp.where(hit, 1.0, named)
        weight = jnp.where(hit, weights_v[j : j + 1, :], weight)
    row = lax.broadcasted_iota(jnp.int32, (LANES, LANES), 0)
    col = lax.broadcasted_iota(jnp.int32, (LANES, LANES), 1)
    before = jnp.where((row // seqs == col // seqs) & (row < col), 1.0, 0.0).astype(bf16)
    count = jnp.dot(named.astype(bf16), before, preferred_element_type=f32)
    first = jnp.where(count < 0.5, named, 0.0)
    second = named - first
    hi = weight.astype(bf16).astype(f32)
    lo = weight - hi
    sel = jnp.concatenate([first, second], axis=0).astype(bf16)
    sel_hi = jnp.concatenate([first * hi, second * hi], axis=0).astype(bf16)
    sel_lo = jnp.concatenate([first * lo, second * lo], axis=0).astype(bf16)
    lines = slots * 2 * pieces
    r2 = lax.broadcasted_iota(jnp.int32, (lines, 2 * experts), 0)
    c2 = lax.broadcasted_iota(jnp.int32, (lines, 2 * experts), 1)
    rank = r2 // (4 * pieces)
    dz = jnp.where(rank % 2 == 1, (rank + 1) // 2, -(rank // 2))
    dc = (r2 // (2 * pieces)) % 2
    goal = (((z + nz + dz) % nz) * NX + px) * 2 + jnp.where(dc == 0, c, 1 - c)
    choose = jnp.where(c2 == goal + ((r2 // pieces) % 2) * experts, 1.0, 0.0).astype(bf16)
    r3 = lax.broadcasted_iota(jnp.int32, (lines, LANES), 0)
    c3 = lax.broadcasted_iota(jnp.int32, (lines, LANES), 1)
    same = (r3 % pieces) == (c3 // seqs)

    def spread(matrix):
        return jnp.where(same, jnp.dot(choose, matrix, preferred_element_type=f32), 0.0)

    pick_v[...] = spread(sel).astype(bf16)
    pull_hi_v[...] = spread(sel_hi).T.astype(bf16)
    pull_lo_v[...] = spread(sel_lo).T.astype(bf16)

    half = 2 * per
    order = jnp.where((row // half == col % pieces) & (row % half == col // pieces), 1.0, 0.0).astype(bf16)
    disorder = jnp.where((col // half == row % pieces) & (col % half == row // pieces), 1.0, 0.0).astype(bf16)

    ready(tokens_v, gain_in_v)
    xf = tokens_v[...].astype(f32)
    normed = (xf * rms(xf) * gain_in_v[...]).astype(bf16)
    ready(wq_v, wk_v, wv_v)
    key_dim = wq_v.shape[1]
    query = jnp.dot(normed, wq_v[...], preferred_element_type=f32) * key_dim ** (-0.5)
    keys = jnp.dot(normed, wk_v[...], preferred_element_type=f32)
    values = jnp.dot(normed, wv_v[...], preferred_element_type=f32)
    ready(wi_v, wf_v, bi_v, bf_v, scale_v)
    nf = normed.astype(f32)
    in_pre = jnp.sum(nf * wi_v[...].astype(f32), axis=-1, keepdims=True) + bi_v[...]
    fg = jnp.sum(nf * wf_v[...].astype(f32), axis=-1, keepdims=True) + bf_v[...]
    forget_log = jnp.minimum(fg, 0.0) - jnp.log1p(jnp.exp(-jnp.abs(fg)))
    tr = lax.broadcasted_iota(jnp.int32, (seqs, seqs), 0)
    tc = lax.broadcasted_iota(jnp.int32, (seqs, seqs), 1)
    log_scale = jnp.sum(
        jnp.where(tr == tc, jnp.broadcast_to(scale_v[...], (seqs, seqs)), 0.0), axis=-1, keepdims=True
    )
    carried = forget_log + log_scale
    new_max = jnp.maximum(carried, in_pre)
    carry_weight = jnp.exp(carried - new_max)
    fresh_weight = jnp.exp(in_pre - new_max)
    match = jnp.sum(query * keys, axis=-1, keepdims=True)
    turned = query.T
    ready(memory_v)
    for s in range(seqs):
        recall_v[s : s + 1, :] = jnp.sum(turned[:, s : s + 1] * memory_v[s], axis=0, keepdims=True)
    read = carry_weight * recall_v[...] + (fresh_weight * match) * values
    ready(head_gain_v, wo_v)
    headout = (read * rms(read) * head_gain_v[...]).astype(bf16)
    mix_v[y] = jnp.dot(headout, wo_v[...], preferred_element_type=f32).astype(bf16)

    pl.semaphore_wait(barrier, NY - 1 + slots - jnp.where(mine, 1, 0))

    def to_peers(ref, send_sem, recv_sem):
        copies = []
        for step in range(1, NY):
            copy = pltpu.make_async_remote_copy(
                src_ref=ref.at[y], dst_ref=ref.at[y], send_sem=send_sem.at[step], recv_sem=recv_sem.at[step],
                device_id=(me, peer(step)), device_id_type=MESH,
            )
            copy.start()
            copies.append(copy)
        for step in range(1, NY):
            source = peer(NY - step)
            pltpu.make_async_remote_copy(
                src_ref=ref.at[source], dst_ref=ref.at[source], send_sem=send_sem.at[step],
                recv_sem=recv_sem.at[step], device_id=(me, peer(step)), device_id_type=MESH,
            ).wait_recv()
        return copies

    mix_copies = to_peers(mix_v, mix_send, mix_recv)
    mixed = mix_v[0].astype(f32)
    for i in range(1, NY):
        mixed = mixed + mix_v[i].astype(f32)
    ready(gain_out_v, gain_ffn_v)
    resid = (xf + mixed * rms(mixed) * gain_out_v[...]).astype(bf16)
    rf = resid.astype(f32)
    resid_v[...] = rf
    ffn_in = (rf * rms(rf) * gain_ffn_v[...]).astype(bf16)

    def stacked(array):
        return jnp.concatenate([array[:, k * LANES : (k + 1) * LANES] for k in range(pieces)], axis=0)

    message = jnp.dot(pick_v[...], stacked(ffn_in), preferred_element_type=f32).astype(bf16)
    msg_v[...] = message.reshape(slots, 2 * pieces, LANES)

    def away(slot, src, dst, sign, send_sem, recv_sem):
        return pltpu.make_async_remote_copy(
            src_ref=src, dst_ref=dst, send_sem=send_sem, recv_sem=recv_sem,
            device_id=(target(slot, sign), y), device_id_type=MESH,
        )

    own = away(0, msg_v.at[0], rows_v.at[y, 0], 1, self_send, self_recv)

    @pl.when(jnp.logical_not(mine))
    def _():
        own.start()

    @pl.when(mine)
    def _():
        rows_v[y, 0] = msg_v[0]

    for slot in range(1, slots):
        away(slot, msg_v.at[slot], rows_v.at[y, slot], 1, out_send, in_recv.at[slot // per]).start()

    ready(eg_v, eu_v, ed_v)

    def arrive(g):
        lo_slot = 1 if g == 0 else g * per
        region = rows_v.at[y, pl.ds(lo_slot, (g + 1) * per - lo_slot)]
        away(0, region, region, 1, out_send, in_recv.at[g]).wait_recv()
        if g == 0:

            @pl.when(jnp.logical_not(mine))
            def _():
                own.wait_recv()

        for step in range(1, NY):
            piece = rows_v.at[y, pl.ds(g * per, per)]
            pltpu.make_async_remote_copy(
                src_ref=piece, dst_ref=piece, send_sem=gat_send, recv_sem=gat_recv.at[step, g],
                device_id=(me, peer(step)), device_id_type=MESH,
            ).start()

    def expert(g):
        for step in range(1, NY):
            source = peer(NY - step)
            piece = rows_v.at[source, pl.ds(g * per, per)]
            pltpu.make_async_remote_copy(
                src_ref=piece, dst_ref=piece, send_sem=gat_send, recv_sem=gat_recv.at[step, g],
                device_id=(me, peer(step)), device_id_type=MESH,
            ).wait_recv()
        side = jnp.concatenate(
            [rows_v[i, g * per : (g + 1) * per].reshape(per * 2 * pieces, LANES) for i in range(NY)], axis=1
        )
        sorted_rows = jnp.dot(order, side, preferred_element_type=f32).astype(bf16)
        inputs = jnp.concatenate(
            [
                jnp.concatenate(
                    [sorted_rows[k * half : (k + 1) * half, i * LANES : (i + 1) * LANES] for k in range(pieces)],
                    axis=1,
                )
                for i in range(NY)
            ],
            axis=0,
        )
        gate = jnp.dot(inputs, eg_v[...], preferred_element_type=f32)
        up = jnp.dot(inputs, eu_v[...], preferred_element_type=f32)
        act = (jax.nn.silu(gate) * up).astype(bf16)
        part = jnp.dot(act, ed_v[...], preferred_element_type=f32).astype(bf16)
        for i in range(NY):
            part_v[g, i] = part[i * half : (i + 1) * half, :]
        for step in range(1, NY):
            pltpu.make_async_remote_copy(
                src_ref=part_v.at[g, peer(step)], dst_ref=red_v.at[g, step], send_sem=red_send,
                recv_sem=red_recv.at[step, g], device_id=(me, peer(step)), device_id_type=MESH,
            ).start()

    back_own = away(0, back_v.at[0], home_v.at[0], -1, ret_self_send, ret_self_recv)

    def give_back(g):
        total = part_v[g, y].astype(f32)
        for step in range(1, NY):
            pltpu.make_async_remote_copy(
                src_ref=part_v.at[g, peer(step)], dst_ref=red_v.at[g, step], send_sem=red_send,
                recv_sem=red_recv.at[step, g], device_id=(me, peer(step)), device_id_type=MESH,
            ).wait_recv()
        for step in range(1, NY):
            total = total + red_v[g, step].astype(f32)
        lined = jnp.dot(disorder, stacked(total.astype(bf16)), preferred_element_type=f32).astype(bf16)
        back_v[g * per : (g + 1) * per] = lined.reshape(per, 2 * pieces, LANES)
        for slot in range(g * per, (g + 1) * per):
            if slot == 0:

                @pl.when(jnp.logical_not(mine))
                def _():
                    back_own.start()

                @pl.when(mine)
                def _():
                    home_v[0] = back_v[0]

            else:
                away(slot, back_v.at[slot], home_v.at[slot], -1, ret_send, ret_recv.at[g]).start()

    for step in range(CHUNKS + 2):
        if step < CHUNKS:
            arrive(step)
        if 1 <= step <= CHUNKS:
            expert(step - 1)
        if step >= 2:
            give_back(step - 2)

    routed = jnp.zeros((LANES, LANES), f32)
    for g in range(CHUNKS):
        lo_slot = 1 if g == 0 else g * per
        region = home_v.at[pl.ds(lo_slot, (g + 1) * per - lo_slot)]
        away(0, region, region, -1, ret_send, ret_recv.at[g]).wait_recv()
        if g == 0:

            @pl.when(jnp.logical_not(mine))
            def _():
                back_own.wait_recv()

        block = home_v[g * per : (g + 1) * per].reshape(per * 2 * pieces, LANES)
        span = slice(g * per * 2 * pieces, (g + 1) * per * 2 * pieces)
        routed = routed + jnp.dot(pull_hi_v[:, span], block, preferred_element_type=f32)
        routed = routed + jnp.dot(pull_lo_v[:, span], block, preferred_element_type=f32)
    flat = jnp.concatenate([routed[k * seqs : (k + 1) * seqs, :] for k in range(pieces)], axis=1)
    last_v[y] = flat.astype(bf16)
    last_copies = to_peers(last_v, last_send, last_recv)
    total = last_v[0].astype(f32)
    for i in range(1, NY):
        total = total + last_v[i].astype(f32)
    total_v[...] = total * rms(total)
    ready(gain_last_v)
    quarter = width // NY
    mark = pl.ds(pl.multiple_of(y * quarter, quarter), quarter)
    out_ref[...] = (resid_v[:, mark] + total_v[:, mark] * gain_last_v[...]).astype(bf16)

    for copy in mix_copies + last_copies:
        copy.wait_send()
    rest = msg_v.at[pl.ds(1, slots - 1)]
    away(0, rest, rest, 1, out_send, self_recv).wait_send()
    rest = back_v.at[pl.ds(1, slots - 1)]
    away(0, rest, rest, 1, ret_send, self_recv).wait_send()

    @pl.when(jnp.logical_not(mine))
    def _():
        own.wait_send()
        back_own.wait_send()

    everything = rows_v.at[pl.ds(0, NY - 1)]
    away(0, everything, everything, 1, gat_send, self_recv).wait_send()
    everything = red_v.at[:, pl.ds(1, NY - 1)]
    away(0, everything, everything, 1, red_send, self_recv).wait_send()


def per_device(
    nz, tokens, memory, log_scale, mix_gain_in, w_query, w_key, w_value, w_igate, w_fgate, igate_bias, fgate_bias,
    head_gain, w_output, mix_gain_out, ffn_gain_in, routes, route_weights, expert_gate, expert_up, expert_down,
    ffn_gain_out,
):
    f32, bf16 = jnp.float32, jnp.bfloat16
    seqs, width = tokens.shape
    pieces = width // LANES
    key_dim, value_dim = memory.shape[2:]
    slots = 2 * nz
    per = slots // CHUNKS
    lines = slots * 2 * pieces
    hidden = expert_gate.shape[2]
    operands = [
        tokens, memory[:, 0], log_scale.T, mix_gain_in[None], w_query, w_key, w_value, w_igate.T, w_fgate.T,
        igate_bias[None], fgate_bias[None], head_gain[None], w_output, mix_gain_out[None], ffn_gain_in[None],
        jnp.tile(routes.T, (1, LANES // seqs)), jnp.tile(route_weights.T, (1, LANES // seqs)),
        expert_gate[0], expert_up[0], expert_down[0], ffn_gain_out[None],
    ]
    dma, vmem = pltpu.SemaphoreType.DMA, pltpu.VMEM
    scratch = [vmem(a.shape, a.dtype) for a in operands] + [
        vmem((seqs, value_dim), f32),
        vmem((NY, seqs, width), bf16),
        vmem((lines, LANES), bf16),
        vmem((LANES, lines), bf16),
        vmem((LANES, lines), bf16),
        vmem((slots, 2 * pieces, LANES), bf16),
        vmem((NY, slots, 2 * pieces, LANES), bf16),
        vmem((CHUNKS, NY, 2 * per, width), bf16),
        vmem((CHUNKS, NY, 2 * per, width), bf16),
        vmem((slots, 2 * pieces, LANES), bf16),
        vmem((slots, 2 * pieces, LANES), bf16),
        vmem((NY, seqs, width), bf16),
        vmem((seqs, width), f32),
        vmem((seqs, width), f32),
        dma((len(operands),)), dma((NY,)), dma((NY,)), dma, dma, dma((CHUNKS,)), dma, dma, dma((NY, CHUNKS)),
        dma, dma((NY, CHUNKS)), dma, dma, dma((CHUNKS,)), dma, dma((NY,)), dma((NY,)),
    ]
    return pl.pallas_call(
        functools.partial(kernel, nz),
        out_shape=jax.ShapeDtypeStruct((seqs, width // NY), bf16),
        in_specs=[pl.BlockSpec(memory_space=pltpu.HBM)] * len(operands),
        out_specs=pl.BlockSpec(memory_space=pltpu.VMEM),
        scratch_shapes=scratch,
        compiler_params=pltpu.CompilerParams(collective_id=0, has_side_effects=True, vmem_limit_bytes=32 << 20),
    )(*operands)


def solution(mesh):
    nz = mesh.shape["ep"] // (2 * NX)
    return jax.shard_map(
        functools.partial(per_device, nz),
        mesh=mesh,
        in_specs=(
            P("ep", None), P("ep", "tp", None, None), P("ep", "tp"), P(), P(None, "tp"), P(None, "tp"),
            P(None, "tp"), P(None, "tp"), P(None, "tp"), P("tp"), P("tp"), P("tp"), P("tp", None), P(), P(),
            P("ep", None), P("ep", None), P("ep", None, "tp"), P("ep", None, "tp"), P("ep", "tp", None), P("tp"),
        ),
        out_specs=P("ep", "tp"),
        check_vma=False,
    )
```

time: 116 us -> 80.9 us (0.70)
  blocking collectives: 65.9 us -> 0 us
  Pallas kernels: 0 us -> 61.8 us
  waiting for transfers between devices: 18.9 us -> 0 us
  starting transfers between devices: 13.5 us -> 0 us
  local copies, waits for them, and re-layouts: 4.28 us -> 17 us
  matrix products: 6.99 us -> 0 us
  other arithmetic: 2.92 us -> 0 us
    all_to_all x4 -> x0, blocking collectives: 65.9 us -> none  [the longest x1 37.1 us: per_device(): lax.all_to_all(outbound, 'ep', split_axis=0, concat_axis=0, tiled=True)]
    pallas_call x0 -> x1, Pallas kernels: none -> 61.8 us  [per_device(): pl.pallas_call(functools.partial(kernel, nz), out_shape=jax.ShapeDtypeStr...]
    all_to_all x2 -> x0, waiting for transfers between devices: 18.9 us -> none  [the longest x1 15.8 us: per_device(): lax.all_to_all(done, 'ep', split_axis=0, concat_axis=0, tiled=True)]
    unnamed x28 -> x35, local copies, waits for them, and re-layouts: 0.24 us -> 15.5 us
    all_to_all x2 -> x0, starting transfers between devices: 13.5 us -> none  [the longest x1 8.52 us: per_device(): lax.all_to_all(done, 'ep', split_axis=0, concat_axis=0, tiled=True)]
    dot_general x10 -> x0, matrix products: 6.99 us -> none  [the longest x1 1.94 us: per_device(): jnp.einsum('secf,efd->secd', act, expert_down, preferred_element_type=f32)]
    reduce_sum x9 -> x0, other arithmetic: 1.87 us -> none  [the longest x3 1.34 us: rms_scale(): return lax.rsqrt(jnp.mean(values * values, axis=-1, keepdims=True) + EPS)]
    another operation x1 -> x4, local copies, waits for them, and re-layouts: 0.05 us -> 1.53 us  [the longest x2 0.77 us: per_device(): jnp.tile(routes.T, (1, LANES // seqs))]
  transfers between devices with their start and end apart: 2 -> 0, of which waited for: 2 -> 0; matrix products, arithmetic and copies ran while one was open for 2% -> 0% of each run, Pallas kernels for 0% -> 0%
where the time goes in v1:
time: 80.9 us; the launch traced here: 80.2 us
  Pallas kernels  61.8 us (76%)
  local copies, waits for them, and re-layouts  17 us (21%)
  between operations  1.34 us (2%)
    pallas_call x1, Pallas kernels, per_device(): pl.pallas_call(functools.partial(kernel, nz), out_shape=jax.ShapeDtypeStr...  61.8 us
    unnamed x35, local copies, waits for them, and re-layouts  15.5 us

profile of v1, /device:TPU:1, one launch (start us, length us, event | category | flops | bytes accessed | tf_op | source)
XLA Modules:
  0.0 80.2 jit_solution(6342294801859548162)
XLA Ops:
  0.0 0.7 tile.20
  0.7 0.1 tile.21.weights_h
  0.8 0.7 tile.8
  1.5 0.1 tile.9.routes_h
  2.8 0.0 copy-start
  2.8 1.6 %copy-done = f32[16,1,128,256]{3,2,1,0:T(8,128)S(1)} copy-done((f32[16,1,128,256]{3,2,1,0:T(8,128)S(1)}, f32[16,1,128,256]{3,2,1,0:T(8,128)}, u32[]{:S(2)}) %copy-start) | copy-done | bytes 2097176
  4.4 0.0 copy-start.1
  4.4 1.0 %copy-done.1 = bf16[1024,256]{1,0:T(8,128)(2,1)S(1)} copy-done((bf16[1024,256]{1,0:T(8,128)(2,1)S(1)}, bf16[1024,256]{1,0:T(8,128)(2,1)}, u32[]{:S(2)}) %copy-start.1) | copy-done | bytes 524312
  5.5 0.0 copy-start.2
  5.5 1.0 %copy-done.2 = bf16[256,1024]{1,0:T(8,128)(2,1)S(1)} copy-done((bf16[256,1024]{1,0:T(8,128)(2,1)S(1)}, bf16[256,1024]{1,0:T(8,128)(2,1)}, u32[]{:S(2)}) %copy-start.2) | copy-done | bytes 524312
  6.5 0.0 copy-start.3
  6.5 1.0 %copy-done.3 = bf16[1,1024,256]{2,1,0:T(8,128)(2,1)S(1)} copy-done((bf16[1,1024,256]{2,1,0:T(8,128)(2,1)S(1)}, bf16[1,1024,256]{2,1,0:T(8,128)(2,1)}, u32[]{:S(2)}) %copy-start.3) | copy-done | bytes 524312
  7.6 0.0 copy-start.4
  7.6 1.0 %copy-done.4 = bf16[1,1024,256]{2,1,0:T(8,128)(2,1)S(1)} copy-done((bf16[1,1024,256]{2,1,0:T(8,128)(2,1)S(1)}, bf16[1,1024,256]{2,1,0:T(8,128)(2,1)}, u32[]{:S(2)}) %copy-start.4) | copy-done | bytes 524312
  8.6 0.0 copy-start.5
  8.6 1.0 %copy-done.5 = bf16[1,256,1024]{2,1,0:T(8,128)(2,1)S(1)} copy-done((bf16[1,256,1024]{2,1,0:T(8,128)(2,1)S(1)}, bf16[1,256,1024]{2,1,0:T(8,128)(2,1)}, u32[]{:S(2)}) %copy-start.5) | copy-done | bytes 524312
  9.6 0.0 copy-start.6
  9.6 0.9 %copy-done.6 = bf16[1024,128]{1,0:T(8,128)(2,1)S(1)} copy-done((bf16[1024,128]{1,0:T(8,128)(2,1)S(1)}, bf16[1024,128]{1,0:T(8,128)(2,1)}, u32[]{:S(2)}) %copy-start.6) | copy-done | bytes 262168
  10.6 0.0 copy-start.7
  10.6 0.9 %copy-done.7 = bf16[1024,128]{1,0:T(8,128)(2,1)S(1)} copy-done((bf16[1024,128]{1,0:T(8,128)(2,1)S(1)}, bf16[1024,128]{1,0:T(8,128)(2,1)}, u32[]{:S(2)}) %copy-start.7) | copy-done | bytes 262168
  11.5 0.0 copy-start.8
  11.5 0.8 copy-done.8
  12.3 0.0 copy-start.9
  12.3 0.7 copy-done.9
  13.0 0.0 copy-start.10
  13.0 0.7 copy-done.10
  13.7 0.0 copy-start.11
  13.7 0.7 copy-done.11
  14.4 0.0 copy-start.12
  14.4 0.7 copy-done.12
  15.0 0.0 copy-start.13
  15.1 0.7 copy-done.13
  15.7 0.0 copy-start.14
  15.7 0.7 copy-done.14
  16.4 0.0 copy-start.15
  16.4 0.7 copy-done.15
  17.1 0.0 copy-start.16
  17.1 0.7 copy-done.16
  17.8 61.8 %shard_map.199 = bf16[16,256]{1,0:T(8,128)(2,1)S(1)} custom-call(bf16[16,1024]{1,0:T(8,128)(2,1)S(1)} %copy-done.8, f32[16,128,256]{2,1,0:T(8,128)S(1)} %bitcast.18, f32[1,16]{1,0:T(1,128)S(1)} %bitcast.29, f32[1,1024]{1,0:T(1,128)S(1)} %bitcast.22, bf16[1024,128]{1,0:T(8,128)(2,1)S(1)} %copy-done.6, bf16[1024,128]{1,0:T(8,128)(2,1)S(1)} %copy-done.7, ...), custom_call_target="tpu_custom_call" | custom-call | tf_op jit(solution)/shard_map/pallas_call | solution.py:385
  79.6 0.6 copy.25
Async XLA Ops:
  2.8 1.6 %copy-start = (f32[16,1,128,256]{3,2,1,0:T(8,128)S(1)}, f32[16,1,128,256]{3,2,1,0:T(8,128)}, u32[]{:S(2)}) copy-start(f32[16,1,128,256]{3,2,1,0:T(8,128)} %param.22) | copy-start | bytes 6291460
  4.4 1.0 %copy-start.1 = (bf16[1024,256]{1,0:T(8,128)(2,1)S(1)}, bf16[1024,256]{1,0:T(8,128)(2,1)}, u32[]{:S(2)}) copy-start(bf16[1024,256]{1,0:T(8,128)(2,1)} %wv_h.1) | copy-start | bytes 1572868
  5.5 1.0 %copy-start.2 = (bf16[256,1024]{1,0:T(8,128)(2,1)S(1)}, bf16[256,1024]{1,0:T(8,128)(2,1)}, u32[]{:S(2)}) copy-start(bf16[256,1024]{1,0:T(8,128)(2,1)} %wo_h.1) | copy-start | bytes 1572868
  6.5 1.0 %copy-start.3 = (bf16[1,1024,256]{2,1,0:T(8,128)(2,1)S(1)}, bf16[1,1024,256]{2,1,0:T(8,128)(2,1)}, u32[]{:S(2)}) copy-start(bf16[1,1024,256]{2,1,0:T(8,128)(2,1)} %param.38) | copy-start | bytes 1572868
  7.6 1.0 %copy-start.4 = (bf16[1,1024,256]{2,1,0:T(8,128)(2,1)S(1)}, bf16[1,1024,256]{2,1,0:T(8,128)(2,1)}, u32[]{:S(2)}) copy-start(bf16[1,1024,256]{2,1,0:T(8,128)(2,1)} %param.39) | copy-start | bytes 1572868
  8.6 1.0 %copy-start.5 = (bf16[1,256,1024]{2,1,0:T(8,128)(2,1)S(1)}, bf16[1,256,1024]{2,1,0:T(8,128)(2,1)}, u32[]{:S(2)}) copy-start(bf16[1,256,1024]{2,1,0:T(8,128)(2,1)} %param.40) | copy-start | bytes 1572868
  9.6 0.9 %copy-start.6 = (bf16[1024,128]{1,0:T(8,128)(2,1)S(1)}, bf16[1024,128]{1,0:T(8,128)(2,1)}, u32[]{:S(2)}) copy-start(bf16[1024,128]{1,0:T(8,128)(2,1)} %wq_h.1) | copy-start | bytes 786436
  10.6 0.9 %copy-start.7 = (bf16[1024,128]{1,0:T(8,128)(2,1)S(1)}, bf16[1024,128]{1,0:T(8,128)(2,1)}, u32[]{:S(2)}) copy-start(bf16[1024,128]{1,0:T(8,128)(2,1)} %wk_h.1) | copy-start | bytes 786436
  11.5 0.8 copy-start.8
  12.3 0.7 copy-start.9
  13.0 0.7 copy-start.10
  13.7 0.7 copy-start.11
  14.4 0.7 copy-start.12
  15.0 0.7 copy-start.13
  15.7 0.7 copy-start.14
  16.4 0.7 copy-start.15
  17.1 0.7 copy-start.16

commit v2 on v1

v2 whole, which is shorter than its diff:
```python
import functools

import jax
import jax.numpy as jnp
from jax import lax
from jax.experimental import pallas as pl
from jax.experimental.pallas import tpu as pltpu
from jax.sharding import PartitionSpec as P

EPS = 1e-06
MESH = pl.DeviceIdType.MESH
LANES = 128
NX = 4
NY = 4
CHUNKS = 4
ORDER = (0, 1, 3, 2)


def rms(values):
    return lax.rsqrt(jnp.mean(values * values, axis=-1, keepdims=True) + EPS)


def kernel(
    nz,
    tokens_h, memory_h, scale_h, gain_in_h, wq_h, wk_h, wv_h, wi_h, wf_h, bi_s, bf_s,
    head_gain_h, wo_h, gain_out_h, gain_ffn_h, routes_h, weights_h, eg_h, eu_h, ed_h, gain_last_h,
    out_ref,
    tokens_v, memory_v, scale_v, gain_in_v, wq_v, wk_v, wv_v, wi_v, wf_v,
    head_gain_v, wo_v, gain_out_v, gain_ffn_v, routes_v, weights_v, eg_v, eu_v, ed_v, gain_last_v,
    recall_v, mix_v, pick_v, pull_hi_v, pull_lo_v, msg_v, rows_v, part_v, red_v, back_v, home_v, last_v, resid_v, total_v,
    load_sem, mix_send, mix_recv, out_send, self_send, in_recv, gat_send, gat_recv,
    red_send, red_recv, ret_send, ret_recv, last_send, last_recv,
):
    f32, bf16 = jnp.float32, jnp.bfloat16
    seqs, width = tokens_v.shape
    pieces = width // LANES
    slots = 2 * nz
    per = slots // CHUNKS
    experts = nz * NX * 2

    me = lax.axis_index("ep")
    y = lax.axis_index("tp")
    c = me % 2
    x = (me // 2) % NX
    z = me // (2 * NX)
    px = (y + NX - x) % NX
    mine = px == x

    self_slot = z * 2 + c

    def partner(slot):
        return (slot // 2 * NX + px) * 2 + slot % 2

    far = sorted(range(nz), key=lambda off: -min(off, nz - off))
    around = [(z + off) % nz * 2 + (1 - c if other else c) for off in far for other in (1, 0)]

    def peer(step):
        return (y + step) % NY

    pairs = [
        (routes_h, routes_v), (weights_h, weights_v), (tokens_h, tokens_v), (gain_in_h, gain_in_v),
        (wq_h, wq_v), (wk_h, wk_v), (wv_h, wv_v), (wi_h, wi_v), (wf_h, wf_v),
        (scale_h, scale_v), (memory_h, memory_v), (head_gain_h, head_gain_v), (wo_h, wo_v),
        (gain_out_h, gain_out_v), (gain_ffn_h, gain_ffn_v), (eg_h, eg_v), (eu_h, eu_v), (ed_h, ed_v),
        (gain_last_h, gain_last_v),
    ]
    loads = {}
    for i, (src, dst) in enumerate(pairs):
        loads[id(dst)] = pltpu.make_async_copy(src, dst, load_sem.at[i])
        loads[id(dst)].start()

    def ready(*refs):
        for ref in refs:
            loads[id(ref)].wait()

    barrier = pltpu.get_barrier_semaphore()
    stays = [mine & (self_slot == slot) for slot in range(slots)]
    for step in range(1, NY):
        pl.semaphore_signal(barrier, inc=1, device_id=(me, peer(step)), device_id_type=MESH)
    for slot in around[:-1]:
        pl.semaphore_signal(barrier, inc=1, device_id=(partner(slot), y), device_id_type=MESH)

    @pl.when(jnp.logical_not(mine))
    def _():
        pl.semaphore_signal(barrier, inc=1, device_id=(partner(self_slot), y), device_id_type=MESH)

    ready(tokens_v, gain_in_v)
    xf = tokens_v[...].astype(f32)
    normed = (xf * rms(xf) * gain_in_v[...]).astype(bf16)
    ready(wq_v, wk_v, wv_v)
    key_dim = wq_v.shape[1]
    query = jnp.dot(normed, wq_v[...], preferred_element_type=f32) * key_dim ** (-0.5)
    keys = jnp.dot(normed, wk_v[...], preferred_element_type=f32)
    values = jnp.dot(normed, wv_v[...], preferred_element_type=f32)
    ready(wi_v, wf_v, scale_v)
    nf = normed.astype(f32)
    in_pre = jnp.sum(nf * wi_v[...].astype(f32), axis=-1, keepdims=True) + bi_s[0]
    fg = jnp.sum(nf * wf_v[...].astype(f32), axis=-1, keepdims=True) + bf_s[0]
    forget_log = jnp.minimum(fg, 0.0) - jnp.log1p(jnp.exp(-jnp.abs(fg)))
    tr = lax.broadcasted_iota(jnp.int32, (seqs, seqs), 0)
    tc = lax.broadcasted_iota(jnp.int32, (seqs, seqs), 1)
    log_scale = jnp.sum(
        jnp.where(tr == tc, jnp.broadcast_to(scale_v[...], (seqs, seqs)), 0.0), axis=-1, keepdims=True
    )
    carried = forget_log + log_scale
    new_max = jnp.maximum(carried, in_pre)
    carry_weight = jnp.exp(carried - new_max)
    fresh_weight = jnp.exp(in_pre - new_max)
    match = jnp.sum(query * keys, axis=-1, keepdims=True)
    turned = query.T
    ready(memory_v)
    for s in range(seqs):
        recall_v[s : s + 1, :] = jnp.sum(turned[:, s : s + 1] * memory_v[s], axis=0, keepdims=True)
    read = carry_weight * recall_v[...] + (fresh_weight * match) * values
    ready(head_gain_v, wo_v)
    headout = (read * rms(read) * head_gain_v[...]).astype(bf16)
    mix_v[y] = jnp.dot(headout, wo_v[...], preferred_element_type=f32).astype(bf16)

    pl.semaphore_wait(barrier, NY - 1 + slots - jnp.where(mine, 1, 0))

    def to_peers(ref, send_sem, recv_sem):
        copies = []
        for step in (2, 1, 3):
            copy = pltpu.make_async_remote_copy(
                src_ref=ref.at[y], dst_ref=ref.at[y], send_sem=send_sem.at[step], recv_sem=recv_sem.at[step],
                device_id=(me, peer(step)), device_id_type=MESH,
            )
            copy.start()
            copies.append(copy)
        return copies

    def from_peers(ref, send_sem, recv_sem):
        for step in range(1, NY):
            source = peer(NY - step)
            pltpu.make_async_remote_copy(
                src_ref=ref.at[source], dst_ref=ref.at[source], send_sem=send_sem.at[step],
                recv_sem=recv_sem.at[step], device_id=(me, peer(step)), device_id_type=MESH,
            ).wait_recv()

    mix_copies = to_peers(mix_v, mix_send, mix_recv)

    ready(routes_v, weights_v)
    expert_row = lax.broadcasted_iota(jnp.int32, (experts, seqs), 0)
    named = jnp.zeros((experts, seqs), f32)
    weight = jnp.zeros((experts, seqs), f32)
    for j in range(routes_v.shape[0]):
        hit = expert_row == routes_v[j : j + 1, :]
        named = jnp.where(hit, 1.0, named)
        weight = jnp.where(hit, weights_v[j : j + 1, :], weight)
    row = lax.broadcasted_iota(jnp.int32, (LANES, LANES), 0)
    col = lax.broadcasted_iota(jnp.int32, (LANES, LANES), 1)
    before = jnp.where(row[:seqs, :seqs] < col[:seqs, :seqs], 1.0, 0.0).astype(bf16)
    count = jnp.dot(named.astype(bf16), before, preferred_element_type=f32)
    first = jnp.where(count < 0.5, named, 0.0)
    second = named - first
    copies_of = jnp.where(row[:seqs] == col[:seqs] % seqs, 1.0, 0.0).astype(bf16)
    lines = slots * 2 * pieces
    r2 = lax.broadcasted_iota(jnp.int32, (lines, 2 * experts), 0)
    c2 = lax.broadcasted_iota(jnp.int32, (lines, 2 * experts), 1)
    goal = (r2 // (4 * pieces) * NX + px) * 2 + r2 // (2 * pieces) % 2
    choose = jnp.where(c2 == goal + r2 // pieces % 2 * experts, 1.0, 0.0).astype(bf16)
    r3 = lax.broadcasted_iota(jnp.int32, (lines, LANES), 0)
    c3 = lax.broadcasted_iota(jnp.int32, (lines, LANES), 1)
    same = (r3 % pieces) == (c3 // seqs)

    def spread(one, two):
        both = jnp.concatenate([one, two], axis=0).astype(bf16)
        wide = jnp.dot(both, copies_of, preferred_element_type=f32).astype(bf16)
        return jnp.where(same, jnp.dot(choose, wide, preferred_element_type=f32), 0.0)

    pick_v[...] = spread(first, second).astype(bf16)

    from_peers(mix_v, mix_send, mix_recv)
    mixed = mix_v[0].astype(f32)
    for i in range(1, NY):
        mixed = mixed + mix_v[i].astype(f32)
    ready(gain_out_v, gain_ffn_v)
    resid = (xf + mixed * rms(mixed) * gain_out_v[...]).astype(bf16)
    rf = resid.astype(f32)
    resid_v[...] = rf
    ffn_in = (rf * rms(rf) * gain_ffn_v[...]).astype(bf16)

    def stacked(array):
        return jnp.concatenate([array[:, k * LANES : (k + 1) * LANES] for k in range(pieces)], axis=0)

    message = jnp.dot(pick_v[...], stacked(ffn_in), preferred_element_type=f32).astype(bf16)
    msg_v[...] = message.reshape(slots, 2 * pieces, LANES)

    def away(slot, src, dst, send_sem, recv_sem):
        return pltpu.make_async_remote_copy(
            src_ref=src, dst_ref=dst, send_sem=send_sem, recv_sem=recv_sem,
            device_id=(partner(slot), y), device_id_type=MESH,
        )

    own = away(self_slot, msg_v.at[self_slot], rows_v.at[y, self_slot], self_send, in_recv.at[self_slot])
    @pl.when(mine)
    def _():
        rows_v[y, self_slot] = msg_v[self_slot]

    for slot in around[:-1]:
        away(slot, msg_v.at[slot], rows_v.at[y, self_slot], out_send, in_recv.at[self_slot]).start()

    @pl.when(jnp.logical_not(mine))
    def _():
        own.start()

    hi = weight.astype(bf16).astype(f32)
    lo = weight - hi
    pull_hi_v[...] = spread(first * hi, second * hi).T.astype(bf16)
    pull_lo_v[...] = spread(first * lo, second * lo).T.astype(bf16)

    half = 2 * per
    row = lax.broadcasted_iota(jnp.int32, (half * pieces, half * pieces), 0)
    col = lax.broadcasted_iota(jnp.int32, (half * pieces, half * pieces), 1)
    order = jnp.where((row // half == col % pieces) & (row % half == col // pieces), 1.0, 0.0).astype(bf16)
    disorder = jnp.where((col // half == row % pieces) & (col % half == row // pieces), 1.0, 0.0).astype(bf16)

    ready(eg_v, eu_v, ed_v)

    def from_afar(slot, ref, send_sem, recv_sem):
        @pl.when(jnp.logical_not(stays[slot]))
        def _():
            away(slot, ref, ref, send_sem, recv_sem.at[slot]).wait_recv()

    def arrive(g):
        for slot in range(g * per, (g + 1) * per):
            from_afar(slot, rows_v.at[y, slot], out_send, in_recv)
        for step in range(1, NY):
            piece = rows_v.at[y, pl.ds(g * per, per)]
            pltpu.make_async_remote_copy(
                src_ref=piece, dst_ref=piece, send_sem=gat_send, recv_sem=gat_recv.at[step, g],
                device_id=(me, peer(step)), device_id_type=MESH,
            ).start()

    def expert(g):
        for step in range(1, NY):
            source = peer(NY - step)
            piece = rows_v.at[source, pl.ds(g * per, per)]
            pltpu.make_async_remote_copy(
                src_ref=piece, dst_ref=piece, send_sem=gat_send, recv_sem=gat_recv.at[step, g],
                device_id=(me, peer(step)), device_id_type=MESH,
            ).wait_recv()
        side = jnp.concatenate(
            [rows_v[i, g * per : (g + 1) * per].reshape(per * 2 * pieces, LANES) for i in range(NY)], axis=1
        )
        sorted_rows = jnp.dot(order, side, preferred_element_type=f32).astype(bf16)
        inputs = jnp.concatenate(
            [
                jnp.concatenate(
                    [sorted_rows[k * half : (k + 1) * half, i * LANES : (i + 1) * LANES] for k in range(pieces)],
                    axis=1,
                )
                for i in range(NY)
            ],
            axis=0,
        )
        gate = jnp.dot(inputs, eg_v[...], preferred_element_type=f32)
        up = jnp.dot(inputs, eu_v[...], preferred_element_type=f32)
        act = (jax.nn.silu(gate) * up).astype(bf16)
        part = jnp.dot(act, ed_v[...], preferred_element_type=f32).astype(bf16)
        for i in range(NY):
            part_v[g, i] = part[i * half : (i + 1) * half, :]
        for step in range(1, NY):
            pltpu.make_async_remote_copy(
                src_ref=part_v.at[g, peer(step)], dst_ref=red_v.at[g, step], send_sem=red_send,
                recv_sem=red_recv.at[step, g], device_id=(me, peer(step)), device_id_type=MESH,
            ).start()

    def give_back(g):
        total = part_v[g, y].astype(f32)
        for step in range(1, NY):
            pltpu.make_async_remote_copy(
                src_ref=part_v.at[g, peer(step)], dst_ref=red_v.at[g, step], send_sem=red_send,
                recv_sem=red_recv.at[step, g], device_id=(me, peer(step)), device_id_type=MESH,
            ).wait_recv()
        for step in range(1, NY):
            total = total + red_v[g, step].astype(f32)
        lined = jnp.dot(disorder, stacked(total.astype(bf16)), preferred_element_type=f32).astype(bf16)
        back_v[g * per : (g + 1) * per] = lined.reshape(per, 2 * pieces, LANES)
        for slot in range(g * per, (g + 1) * per):
            @pl.when(jnp.logical_not(stays[slot]))
            def _():
                away(slot, back_v.at[slot], home_v.at[self_slot], ret_send, ret_recv.at[self_slot]).start()

            @pl.when(stays[slot])
            def _():
                home_v[slot] = back_v[slot]

    for g in ORDER:
        arrive(g)
    for g in ORDER:
        expert(g)
    for g in ORDER:
        give_back(g)

    routed = jnp.zeros((LANES, LANES), f32)
    for g in ORDER:
        for slot in range(g * per, (g + 1) * per):
            from_afar(slot, home_v.at[slot], ret_send, ret_recv)
        block = home_v[g * per : (g + 1) * per].reshape(per * 2 * pieces, LANES)
        span = slice(g * per * 2 * pieces, (g + 1) * per * 2 * pieces)
        routed = routed + jnp.dot(pull_hi_v[:, span], block, preferred_element_type=f32)
        routed = routed + jnp.dot(pull_lo_v[:, span], block, preferred_element_type=f32)
    flat = jnp.concatenate([routed[k * seqs : (k + 1) * seqs, :] for k in range(pieces)], axis=1)
    last_v[y] = flat.astype(bf16)
    last_copies = to_peers(last_v, last_send, last_recv)
    from_peers(last_v, last_send, last_recv)
    total = last_v[0].astype(f32)
    for i in range(1, NY):
        total = total + last_v[i].astype(f32)
    total_v[...] = total * rms(total)
    ready(gain_last_v)
    quarter = width // NY
    mark = pl.ds(pl.multiple_of(y * quarter, quarter), quarter)
    out_ref[...] = (resid_v[:, mark] + total_v[:, mark] * gain_last_v[...]).astype(bf16)

    for copy in mix_copies + last_copies:
        copy.wait_send()
    rest = msg_v.at[pl.ds(1, slots - 1)]
    away(self_slot, rest, rest, out_send, in_recv.at[0]).wait_send()
    away(self_slot, rest, rest, ret_send, ret_recv.at[0]).wait_send()

    @pl.when(jnp.logical_not(mine))
    def _():
        own.wait_send()
        away(self_slot, msg_v.at[0], msg_v.at[0], ret_send, ret_recv.at[0]).wait_send()

    everything = rows_v.at[pl.ds(0, NY - 1)]
    away(self_slot, everything, everything, gat_send, in_recv.at[0]).wait_send()
    everything = red_v.at[:, pl.ds(1, NY - 1)]
    away(self_slot, everything, everything, red_send, in_recv.at[0]).wait_send()


def per_device(
    nz, tokens, memory, log_scale, mix_gain_in, w_query, w_key, w_value, w_igate, w_fgate, igate_bias, fgate_bias,
    head_gain, w_output, mix_gain_out, ffn_gain_in, routes, route_weights, expert_gate, expert_up, expert_down,
    ffn_gain_out,
):
    f32, bf16 = jnp.float32, jnp.bfloat16
    seqs, width = tokens.shape
    pieces = width // LANES
    key_dim, value_dim = memory.shape[2:]
    slots = 2 * nz
    per = slots // CHUNKS
    lines = slots * 2 * pieces
    hidden = expert_gate.shape[2]
    operands = [
        tokens, memory[:, 0], log_scale.T, mix_gain_in[None], w_query, w_key, w_value, w_igate.T, w_fgate.T,
        igate_bias, fgate_bias, head_gain[None], w_output, mix_gain_out[None], ffn_gain_in[None],
        routes.T, route_weights.T,
        expert_gate[0], expert_up[0], expert_down[0], ffn_gain_out[None],
    ]
    dma, vmem = pltpu.SemaphoreType.DMA, pltpu.VMEM
    scratch = [vmem(a.shape, a.dtype) for a in operands if a.size > 1] + [
        vmem((seqs, value_dim), f32),
        vmem((NY, seqs, width), bf16),
        vmem((lines, LANES), bf16),
        vmem((LANES, lines), bf16),
        vmem((LANES, lines), bf16),
        vmem((slots, 2 * pieces, LANES), bf16),
        vmem((NY, slots, 2 * pieces, LANES), bf16),
        vmem((CHUNKS, NY, 2 * per, width), bf16),
        vmem((CHUNKS, NY, 2 * per, width), bf16),
        vmem((slots, 2 * pieces, LANES), bf16),
        vmem((slots, 2 * pieces, LANES), bf16),
        vmem((NY, seqs, width), bf16),
        vmem((seqs, width), f32),
        vmem((seqs, width), f32),
        dma((len(operands),)), dma((NY,)), dma((NY,)), dma, dma, dma((slots,)), dma, dma((NY, CHUNKS)),
        dma, dma((NY, CHUNKS)), dma, dma((slots,)), dma((NY,)), dma((NY,)),
    ]
    return pl.pallas_call(
        functools.partial(kernel, nz),
        out_shape=jax.ShapeDtypeStruct((seqs, width // NY), bf16),
        in_specs=[pl.BlockSpec(memory_space=pltpu.HBM if a.size > 1 else pltpu.SMEM) for a in operands],
        out_specs=pl.BlockSpec(memory_space=pltpu.VMEM),
        scratch_shapes=scratch,
        compiler_params=pltpu.CompilerParams(collective_id=0, has_side_effects=True, vmem_limit_bytes=67043328),
    )(*operands)


def solution(mesh):
    nz = mesh.shape["ep"] // (2 * NX)
    return jax.shard_map(
        functools.partial(per_device, nz),
        mesh=mesh,
        in_specs=(
            P("ep", None), P("ep", "tp", None, None), P("ep", "tp"), P(), P(None, "tp"), P(None, "tp"),
            P(None, "tp"), P(None, "tp"), P(None, "tp"), P("tp"), P("tp"), P("tp"), P("tp", None), P(), P(),
            P("ep", None), P("ep", None), P("ep", None, "tp"), P("ep", None, "tp"), P("ep", "tp", None), P("tp"),
        ),
        out_specs=P("ep", "tp"),
        check_vma=False,
    )
```

time: 80.9 us -> 59.4 us (0.73)
  local copies, waits for them, and re-layouts: 17 us -> 1.3 us
  Pallas kernels: 61.8 us -> 56.6 us
    unnamed x35 -> x1, local copies, waits for them, and re-layouts: 15.5 us -> 1.3 us
    pallas_call x1, Pallas kernels: 61.8 us -> 56.6 us  [per_device(): pl.pallas_call(functools.partial(kernel, nz), out_shape=jax.ShapeDtypeStr...]
    another operation x4 -> x0, local copies, waits for them, and re-layouts: 1.53 us -> none  [the longest x2 0.77 us: per_device(): jnp.tile(routes.T, (1, LANES // seqs))]
where the time goes in v2:
time: 59.4 us; the launch traced here: 59.2 us
  Pallas kernels  56.6 us (95%)
  local copies, waits for them, and re-layouts  1.3 us (2%)
  between operations  1.3 us (2%)
    pallas_call x1, Pallas kernels, per_device(): pl.pallas_call(functools.partial(kernel, nz), out_shape=jax.ShapeDtypeStr...  56.6 us
    unnamed x1, local copies, waits for them, and re-layouts  1.3 us

profile of v2, /device:TPU:1, one launch (start us, length us, event | category | flops | bytes accessed | tf_op | source)
XLA Modules:
  0.0 59.2 jit_solution(8761876370033091994)
XLA Ops:
  1.3 56.6 %shard_map.199 = bf16[16,256]{1,0:T(8,128)(2,1)} custom-call(bf16[16,1024]{1,0:T(8,128)(2,1)} %tokens_h.1, f32[16,128,256]{2,1,0:T(8,128)} %bitcast.14, f32[1,16]{1,0:T(1,128)} %bitcast.27, f32[1,1024]{1,0:T(1,128)} %bitcast.18, bf16[1024,128]{1,0:T(8,128)(2,1)} %wq_h.1, bf16[1024,128]{1,0:T(8,128)(2,1)} %wk_h.1, bf16[1024,256]{1,0:T(8,128)(2,1)} %wv_h.1, ...), custom_call_target="tpu_custom_call" | custom-call | tf_op jit(solution)/shard_map/pallas_call | solution.py:372
  57.9 1.3 %copy.25 = bf16[16,256]{1,0:T(8,128)(2,1)} copy(bf16[16,256]{1,0:T(8,128)(2,1)} %shard_map.199) | data formatting | bytes 16384

commit v3 on v2

--- a/solution.py
+++ b/solution.py
@@ -13,7 +13,8 @@
 NX = 4
 NY = 4
 CHUNKS = 4
-ORDER = (0, 1, 3, 2)
+VMEM_LIMIT = 67043328 - 65536
+TURNS = ((0, 1, 3, 2), (0, 1, 3, 2), (2, 3, 0, 1), (3, 2, 0, 1))
 
 
 def rms(values):
@@ -74,7 +75,6 @@
             loads[id(ref)].wait()
 
     barrier = pltpu.get_barrier_semaphore()
-    stays = [mine & (self_slot == slot) for slot in range(slots)]
     for step in range(1, NY):
         pl.semaphore_signal(barrier, inc=1, device_id=(me, peer(step)), device_id_type=MESH)
     for slot in around[:-1]:
@@ -218,12 +218,12 @@
     ready(eg_v, eu_v, ed_v)
 
     def from_afar(slot, ref, send_sem, recv_sem):
-        @pl.when(jnp.logical_not(stays[slot]))
+        @pl.when(jnp.logical_not(mine & (self_slot == slot)))
         def _():
             away(slot, ref, ref, send_sem, recv_sem.at[slot]).wait_recv()
 
     def arrive(g):
-        for slot in range(g * per, (g + 1) * per):
+        for slot in [g * per + i for i in range(per)]:
             from_afar(slot, rows_v.at[y, slot], out_send, in_recv)
         for step in range(1, NY):
             piece = rows_v.at[y, pl.ds(g * per, per)]
@@ -241,7 +241,7 @@
                 device_id=(me, peer(step)), device_id_type=MESH,
             ).wait_recv()
         side = jnp.concatenate(
-            [rows_v[i, g * per : (g + 1) * per].reshape(per * 2 * pieces, LANES) for i in range(NY)], axis=1
+            [rows_v[i, pl.ds(g * per, per)].reshape(per * 2 * pieces, LANES) for i in range(NY)], axis=1
         )
         sorted_rows = jnp.dot(order, side, preferred_element_type=f32).astype(bf16)
         inputs = jnp.concatenate(
@@ -276,25 +276,29 @@
         for step in range(1, NY):
             total = total + red_v[g, step].astype(f32)
         lined = jnp.dot(disorder, stacked(total.astype(bf16)), preferred_element_type=f32).astype(bf16)
-        back_v[g * per : (g + 1) * per] = lined.reshape(per, 2 * pieces, LANES)
-        for slot in range(g * per, (g + 1) * per):
-            @pl.when(jnp.logical_not(stays[slot]))
+        back_v[pl.ds(g * per, per)] = lined.reshape(per, 2 * pieces, LANES)
+        for slot in [g * per + i for i in range(per)]:
+            here = mine & (self_slot == slot)
+
+            @pl.when(jnp.logical_not(here))
             def _():
                 away(slot, back_v.at[slot], home_v.at[self_slot], ret_send, ret_recv.at[self_slot]).start()
 
-            @pl.when(stays[slot])
+            @pl.when(here)
             def _():
                 home_v[slot] = back_v[slot]
 
-    for g in ORDER:
+    group = z // (nz // CHUNKS)
+    turn = [sum(jnp.where(group == k, order_k[i], 0) for k, order_k in enumerate(TURNS)) for i in range(CHUNKS)]
+    for g in turn:
         arrive(g)
-    for g in ORDER:
+    for g in turn:
         expert(g)
-    for g in ORDER:
+    for g in turn:
         give_back(g)
 
     routed = jnp.zeros((LANES, LANES), f32)
-    for g in ORDER:
+    for g in range(CHUNKS):
         for slot in range(g * per, (g + 1) * per):
             from_afar(slot, home_v.at[slot], ret_send, ret_recv)
         block = home_v[g * per : (g + 1) * per].reshape(per * 2 * pieces, LANES)
@@ -371,11 +375,11 @@
     ]
     return pl.pallas_call(
         functools.partial(kernel, nz),
-        out_shape=jax.ShapeDtypeStruct((seqs, width // NY), bf16),
+        out_shape=vmem((seqs, width // NY), bf16),
         in_specs=[pl.BlockSpec(memory_space=pltpu.HBM if a.size > 1 else pltpu.SMEM) for a in operands],
         out_specs=pl.BlockSpec(memory_space=pltpu.VMEM),
         scratch_shapes=scratch,
-        compiler_params=pltpu.CompilerParams(collective_id=0, has_side_effects=True, vmem_limit_bytes=67043328),
+        compiler_params=pltpu.CompilerParams(collective_id=0, has_side_effects=True, vmem_limit_bytes=VMEM_LIMIT),
     )(*operands)
 
 

time: 59.4 us -> 57.6 us (0.970)
  Pallas kernels: 56.6 us -> 55.5 us
  local copies, waits for them, and re-layouts: 1.3 us -> 0.6 us
    pallas_call x1, Pallas kernels: 56.6 us -> 55.5 us  [per_device(): pl.pallas_call(functools.partial(kernel, nz), out_shape=vmem((seqs, width...]
    unnamed x1, local copies, waits for them, and re-layouts: 1.3 us -> 0.6 us
where the time goes in v3:
time: 57.6 us; the launch traced here: 57.4 us
  Pallas kernels  55.5 us (96%)
  between operations  1.3 us (2%)
  local copies, waits for them, and re-layouts  0.6 us (1%)
    pallas_call x1, Pallas kernels, per_device(): pl.pallas_call(functools.partial(kernel, nz), out_shape=vmem((seqs, width...  55.5 us

profile of v3, /device:TPU:1, one launch (start us, length us, event | category | flops | bytes accessed | tf_op | source)
XLA Modules:
  0.0 57.4 jit_solution(2431917507545759226)
XLA Ops:
  1.3 55.5 %shard_map.199 = bf16[16,256]{1,0:T(8,128)(2,1)S(1)} custom-call(bf16[16,1024]{1,0:T(8,128)(2,1)} %tokens_h.1, f32[16,128,256]{2,1,0:T(8,128)} %bitcast.14, f32[1,16]{1,0:T(1,128)} %bitcast.27, f32[1,1024]{1,0:T(1,128)} %bitcast.18, bf16[1024,128]{1,0:T(8,128)(2,1)} %wq_h.1, bf16[1024,128]{1,0:T(8,128)(2,1)} %wk_h.1, bf16[1024,256]{1,0:T(8,128)(2,1)} %wv_h.1, ...), custom_call_target="tpu_custom_call" | custom-call | tf_op jit(solution)/shard_map/pallas_call | solution.py:376
  56.8 0.6 %copy.23 = bf16[16,256]{1,0:T(8,128)(2,1)} copy(bf16[16,256]{1,0:T(8,128)(2,1)S(1)} %shard_map.199) | data formatting | bytes 16384

commit v4 on v3

--- a/solution.py
+++ b/solution.py
@@ -197,8 +197,17 @@
     def _():
         rows_v[y, self_slot] = msg_v[self_slot]
 
-    for slot in around[:-1]:
-        away(slot, msg_v.at[slot], rows_v.at[y, self_slot], out_send, in_recv.at[self_slot]).start()
+    def depart(slots_in_turn):
+        for slot in slots_in_turn:
+            away(slot, msg_v.at[slot], rows_v.at[y, self_slot], out_send, in_recv.at[self_slot]).start()
+
+    @pl.when(z < nz // 2)
+    def _():
+        depart(around[:-1])
+
+    @pl.when(z >= nz // 2)
+    def _():
+        depart(around[-2::-1])
 
     @pl.when(jnp.logical_not(mine))
     def _():

time: 57.6 us -> 56.8 us (0.986)
  Pallas kernels: 55.5 us -> 54.8 us
    pallas_call x1, Pallas kernels: 55.5 us -> 54.8 us  [per_device(): pl.pallas_call(functools.partial(kernel, nz), out_shape=vmem((seqs, width...]
where the time goes in v4:
time: 56.8 us; the launch traced here: 56.7 us
  Pallas kernels  54.8 us (96%)
  between operations  1.3 us (2%)
  local copies, waits for them, and re-layouts  0.6 us (1%)
    pallas_call x1, Pallas kernels, per_device(): pl.pallas_call(functools.partial(kernel, nz), out_shape=vmem((seqs, width...  54.8 us

profile of v4, /device:TPU:1, one launch (start us, length us, event | category | flops | bytes accessed | tf_op | source)
XLA Modules:
  0.0 56.7 jit_solution(4394886147329964178)
XLA Ops:
  1.3 54.8 %shard_map.199 = bf16[16,256]{1,0:T(8,128)(2,1)S(1)} custom-call(bf16[16,1024]{1,0:T(8,128)(2,1)} %tokens_h.1, f32[16,128,256]{2,1,0:T(8,128)} %bitcast.14, f32[1,16]{1,0:T(1,128)} %bitcast.27, f32[1,1024]{1,0:T(1,128)} %bitcast.18, bf16[1024,128]{1,0:T(8,128)(2,1)} %wq_h.1, bf16[1024,128]{1,0:T(8,128)(2,1)} %wk_h.1, bf16[1024,256]{1,0:T(8,128)(2,1)} %wv_h.1, ...), custom_call_target="tpu_custom_call" | custom-call | tf_op jit(solution)/shard_map/pallas_call | solution.py:385
  56.1 0.6 %copy.23 = bf16[16,256]{1,0:T(8,128)(2,1)} copy(bf16[16,256]{1,0:T(8,128)(2,1)S(1)} %shard_map.199) | data formatting | bytes 16384

commit v5 on v4

--- a/solution.py
+++ b/solution.py
@@ -58,6 +58,16 @@
     def peer(step):
         return (y + step) % NY
 
+    barrier = pltpu.get_barrier_semaphore()
+    for step in range(1, NY):
+        pl.semaphore_signal(barrier, inc=1, device_id=(me, peer(step)), device_id_type=MESH)
+    for slot in around[:-1]:
+        pl.semaphore_signal(barrier, inc=1, device_id=(partner(slot), y), device_id_type=MESH)
+
+    @pl.when(jnp.logical_not(mine))
+    def _():
+        pl.semaphore_signal(barrier, inc=1, device_id=(partner(self_slot), y), device_id_type=MESH)
+
     pairs = [
         (routes_h, routes_v), (weights_h, weights_v), (tokens_h, tokens_v), (gain_in_h, gain_in_v),
         (wq_h, wq_v), (wk_h, wk_v), (wv_h, wv_v), (wi_h, wi_v), (wf_h, wf_v),
@@ -73,16 +83,6 @@
     def ready(*refs):
         for ref in refs:
             loads[id(ref)].wait()
-
-    barrier = pltpu.get_barrier_semaphore()
-    for step in range(1, NY):
-        pl.semaphore_signal(barrier, inc=1, device_id=(me, peer(step)), device_id_type=MESH)
-    for slot in around[:-1]:
-        pl.semaphore_signal(barrier, inc=1, device_id=(partner(slot), y), device_id_type=MESH)
-
-    @pl.when(jnp.logical_not(mine))
-    def _():
-        pl.semaphore_signal(barrier, inc=1, device_id=(partner(self_slot), y), device_id_type=MESH)
 
     ready(tokens_v, gain_in_v)
     xf = tokens_v[...].astype(f32)
@@ -301,9 +301,11 @@
     turn = [sum(jnp.where(group == k, order_k[i], 0) for k, order_k in enumerate(TURNS)) for i in range(CHUNKS)]
     for g in turn:
         arrive(g)
-    for g in turn:
+    for g in turn[:-1]:
         expert(g)
-    for g in turn:
+    give_back(turn[0])
+    expert(turn[-1])
+    for g in turn[1:]:
         give_back(g)
 
     routed = jnp.zeros((LANES, LANES), f32)

time: 56.8 us -> 56.8 us (level)
  no operation moved by 1% of the time
where the time goes in v5:
time: 56.8 us; the launch traced here: 56.7 us
  Pallas kernels  54.8 us (96%)
  between operations  1.3 us (2%)
  local copies, waits for them, and re-layouts  0.6 us (1%)
    pallas_call x1, Pallas kernels, per_device(): pl.pallas_call(functools.partial(kernel, nz), out_shape=vmem((seqs, width...  54.8 us

profile of v5, /device:TPU:1, one launch (start us, length us, event | category | flops | bytes accessed | tf_op | source)
XLA Modules:
  0.0 56.7 jit_solution(16270177619499550571)
XLA Ops:
  1.3 54.8 %shard_map.199 = bf16[16,256]{1,0:T(8,128)(2,1)S(1)} custom-call(bf16[16,1024]{1,0:T(8,128)(2,1)} %tokens_h.1, f32[16,128,256]{2,1,0:T(8,128)} %bitcast.14, f32[1,16]{1,0:T(1,128)} %bitcast.27, f32[1,1024]{1,0:T(1,128)} %bitcast.18, bf16[1024,128]{1,0:T(8,128)(2,1)} %wq_h.1, bf16[1024,128]{1,0:T(8,128)(2,1)} %wk_h.1, bf16[1024,256]{1,0:T(8,128)(2,1)} %wv_h.1, ...), custom_call_target="tpu_custom_call" | custom-call | tf_op jit(solution)/shard_map/pallas_call | solution.py:387
  56.1 0.6 %copy.23 = bf16[16,256]{1,0:T(8,128)(2,1)} copy(bf16[16,256]{1,0:T(8,128)(2,1)S(1)} %shard_map.199) | data formatting | bytes 16384
